TPU v7x, 32 devices: a whole 2x2x4 slice. The times are simulated.
32 devices in a mesh: ep: 8 (over z, x), tp: 4 (over y, core).
Axes of the slice: x: 2, y: 2, z: 4, core: 2. Of those that a mesh axis runs over, the one named last changes fastest.
Arguments:
- queries: bfloat16 [2048, 1024], P('ep', 'tp'), may hold values from -256 to 256
- key_rows: bfloat16 [2048, 1024], P('ep', 'tp'), may hold values from -8 to 8
- value_rows: bfloat16 [2048, 1024], P('ep', 'tp'), may hold values from -6 to 6
- head_lambda: float32 [8], P('tp'), may hold values from 0.3 to 0.8
- sub_gain: float32 [128], replicated, may hold values from 0.1 to 1.9
- out_weight: bfloat16 [1024, 2048], P('tp'), may hold values from -0.1875 to 0.1875
- expert_input: bfloat16 [1536, 2048], P('ep'), may hold values from -6 to 6
- norm_gain: float32 [2048], replicated, may hold values from 0.1 to 1.9
- route_ids: int32 [1536, 2], P('ep'), may hold values from 0 to 7, all different within a row; in each aligned block of 192 rows (0 to 191, 192 to 383, ...) at most 80 rows name the same one
- route_weight: float32 [1536, 2], P('ep'), may hold values from 0.25 to 1
- gate_weight: bfloat16 [8, 2048, 3584], P('ep', None, 'tp'), may hold values from -0.125 to 0.125
- up_weight: bfloat16 [8, 2048, 3584], P('ep', None, 'tp'), may hold values from -0.125 to 0.125
- down_weight: bfloat16 [8, 3584, 2048], P('ep', 'tp'), may hold values from -0.09375 to 0.09375
Outputs:
- mixer_out: bfloat16 [2048, 2048], P(('ep', 'tp'))
- expert_out: bfloat16 [1536, 2048], P('ep', 'tp')
Inputs may be any that keep to these rules, and one draw needn't show every extreme that they name: `route_ids`: each row names 2 different experts. In each aligned block of 192 rows no expert is named by more than 80 rows, a bound that some block reaches.
All inputs are finite; a program needn't handle non-finite values.
Results may differ from a plain program's by a relative error of at most 0.014.
Values may be sent and summed in bfloat16 or wider, within the bound.
A program may use at most 256 MiB of HBM per device.

v0:
```python
import jax
import jax.numpy as jnp
from jax import lax
from jax.sharding import PartitionSpec as P

EPS = 1e-06


def mixer_half(queries, key_rows, value_rows, head_lambda, sub_gain, out_weight):
    rows_here = queries.shape[0]
    heads_here = head_lambda.shape[0]
    head_width = queries.shape[1] // (2 * heads_here)
    value_width = value_rows.shape[1] // heads_here
    scaling = head_width ** (-0.5)
    query_blocks = queries.reshape(rows_here, heads_here, 2, head_width)
    query_pos = lax.axis_index("ep") * rows_here + jnp.arange(rows_here, dtype=jnp.int32)
    row_max = jnp.full((heads_here, 2, rows_here), -1e30, jnp.float32)
    key_piece = lax.all_gather(key_rows, "ep", axis=0, tiled=True)
    value_piece = lax.all_gather(value_rows, "ep", axis=0, tiled=True)
    length = key_piece.shape[0]
    key_blocks = key_piece.reshape(length, heads_here, 2, head_width)
    value_blocks = value_piece.reshape(length, heads_here, value_width)
    scores = (
        jnp.einsum("qhmd,khmd->hmqk", query_blocks, key_blocks, preferred_element_type=jnp.float32)
        * scaling
    )
    allowed = query_pos[:, None] >= jnp.arange(length, dtype=jnp.int32)[None, :]
    scores = jnp.where(allowed, scores, -1e30)
    new_max = jnp.maximum(row_max, jnp.max(scores, axis=-1))
    weights = jnp.where(allowed, jnp.exp(scores - new_max[..., None]), 0.0)
    row_total = jnp.sum(weights, axis=-1)
    numerator = jnp.einsum(
        "hmqk,khd->hmqd",
        weights.astype(jnp.bfloat16),
        value_blocks,
        preferred_element_type=jnp.float32,
    )
    row_max, row_total, numerator = (new_max, row_total, numerator)
    per_map = numerator / row_total[..., None]
    contrast = per_map[:, 0] - head_lambda[:, None, None] * per_map[:, 1]
    normed = (
        contrast * lax.rsqrt(jnp.mean(contrast * contrast, axis=-1, keepdims=True) + EPS) * sub_gain
    ).astype(jnp.bfloat16)
    attended = jnp.transpose(normed, (1, 0, 2)).reshape(rows_here, heads_here * value_width)
    return lax.psum_scatter(
        jnp.dot(attended, out_weight, preferred_element_type=jnp.float32).astype(jnp.bfloat16),
        "tp",
        scatter_dimension=0,
        tiled=True,
    )


def expert_half(
    expert_input, norm_gain, route_ids, route_weight, gate_weight, up_weight, down_weight
):
    rows_here, model_width = expert_input.shape
    experts = lax.axis_size("ep")
    top_count = route_ids.shape[1]
    capacity = 5 * top_count * rows_here // (3 * experts)
    slots = experts * capacity
    wide_rows = expert_input.astype(jnp.float32)
    normed = (
        wide_rows
        * lax.rsqrt(jnp.mean(wide_rows * wide_rows, axis=-1, keepdims=True) + EPS)
        * norm_gain
    ).astype(jnp.bfloat16)
    flat_ids = route_ids.reshape(-1)
    onehot = (flat_ids[:, None] == jnp.arange(experts, dtype=jnp.int32)[None, :]).astype(jnp.int32)
    rank_before = jnp.cumsum(onehot, axis=0) - onehot
    slot_index = jnp.sum(rank_before * onehot, axis=1)
    buffer_pos = (flat_ids * capacity + slot_index).reshape(rows_here, top_count)
    matches = buffer_pos[None, :, :] == jnp.arange(slots, dtype=jnp.int32)[:, None, None]
    dispatch = jnp.any(matches, axis=-1).astype(jnp.bfloat16)
    combine = jnp.sum(jnp.where(matches, route_weight[None, :, :], 0.0), axis=-1)
    gate_mat = gate_weight[0]
    up_mat = up_weight[0]
    down_mat = down_weight[0]
    outgoing = jnp.dot(dispatch, normed, preferred_element_type=jnp.float32).astype(jnp.bfloat16)
    arrived = lax.all_to_all(
        outgoing.reshape(experts, capacity, model_width),
        "ep",
        split_axis=0,
        concat_axis=0,
        tiled=True,
    ).reshape(slots, model_width)
    gate_act = jnp.dot(arrived, gate_mat, preferred_element_type=jnp.float32)
    up_act = jnp.dot(arrived, up_mat, preferred_element_type=jnp.float32)
    hidden = (jax.nn.silu(gate_act) * up_act).astype(jnp.bfloat16)
    partial_result = jnp.dot(hidden, down_mat, preferred_element_type=jnp.float32)
    summed = lax.psum_scatter(
        partial_result.astype(jnp.bfloat16), "tp", scatter_dimension=1, tiled=True
    )
    col_count = summed.shape[1]
    returned = lax.all_to_all(
        summed.reshape(experts, capacity, col_count), "ep", split_axis=0, concat_axis=0, tiled=True
    ).reshape(slots, col_count)
    mixed = lax.dot_general(
        combine,
        returned.astype(jnp.float32),
        (((0,), (0,)), ((), ())),
        precision=lax.Precision.HIGHEST,
        preferred_element_type=jnp.float32,
    )
    return mixed.astype(jnp.bfloat16)


def shards(
    queries,
    key_rows,
    value_rows,
    head_lambda,
    sub_gain,
    out_weight,
    expert_input,
    norm_gain,
    route_ids,
    route_weight,
    gate_weight,
    up_weight,
    down_weight,
):
    mixer_out = mixer_half(queries, key_rows, value_rows, head_lambda, sub_gain, out_weight)
    expert_out = expert_half(
        expert_input, norm_gain, route_ids, route_weight, gate_weight, up_weight, down_weight
    )
    return (mixer_out, expert_out)


def solution(mesh):
    placed = (
        P("ep", "tp"),
        P("ep", "tp"),
        P("ep", "tp"),
        P("tp"),
        P(),
        P("tp", None),
        P("ep", None),
        P(),
        P("ep", None),
        P("ep", None),
        P("ep", None, "tp"),
        P("ep", None, "tp"),
        P("ep", "tp", None),
    )
    return jax.shard_map(
        shards,
        mesh=mesh,
        in_specs=placed,
        out_specs=(P(("ep", "tp"), None), P("ep", "tp")),
        check_vma=False,
    )
```

profile of v0, /device:TPU:0, one launch (start us, length us, event | category | flops | bytes accessed | tf_op | source)
XLA Modules:
  0.0 183.7 jit_solution(2173405152536160842)
XLA Ops:
  8.0 0.0 copy-start
  8.0 0.9 copy.43
  8.9 0.1 eq.42
  9.0 0.1 eq.38
  9.2 0.9 reduce-window.6
  10.1 0.2 slice_reduce_fusion
  10.3 0.1 fusion.32
  10.4 0.1 reduce_sum.50
  10.6 0.1 copy.45
  10.6 0.7 multiply_add_fusion
  11.3 0.1 fusion.23
  11.5 1.4 fusion.17
  12.9 3.6 %convolution_convert_fusion = bf16[640,2048]{1,0:T(8,128)(2,1)} fusion(pred[640,192]{0,1:T(8,128)(4,1)S(1)} %fusion.23, bf16[192,2048]{1,0:T(8,128)(2,1)} %param.19, f32[2048]{0:T(1024)} %param.20, f32[192]{0:T(256)S(1)} %add_rsqrt_fusion.1), kind=kOutput, calls=%fused_computation.14 | convolution fusion | flops 506200064 | bytes 3539712 | tf_op jit(solution)/shard_map/dot_general | solution.py:78
  16.5 7.3 %all-to-all-start = ((bf16[8,80,2048]{2,1,0:T(8,128)(2,1)}), bf16[8,80,2048]{2,1,0:T(8,128)(2,1)}, u32[]{:S(2)}, u32[]{:S(2)}) async-start(bf16[8,80,2048]{2,1,0:T(8,128)(2,1)} %bitcast.68), calls=%async_computation.1 | async-start | bytes 5242880 | tf_op jit(solution)/shard_map/all_to_all | solution.py:79
  23.8 0.0 all-gather.3.cloned.1.call-start
  23.8 0.7 all-gather.3.cloned.1.call-update
  24.5 0.0 all-gather.5.cloned.1.call-start
  24.6 0.7 all-gather.5.cloned.1.call-update
  25.3 0.0 reduce-scatter.5.cloned.1.call-start
  25.3 70.7 %all-to-all-done = bf16[8,80,2048]{2,1,0:T(8,128)(2,1)} async-done(((bf16[8,80,2048]{2,1,0:T(8,128)(2,1)}), bf16[8,80,2048]{2,1,0:T(8,128)(2,1)}, u32[]{:S(2)}, u32[]{:S(2)}) %all-to-all-start) | async-done | bytes 2621472 | tf_op jit(solution)/shard_map/all_to_all | solution.py:79
  96.0 7.2 %fusion.10 = f32[640,896]{1,0:T(8,128)} fusion(bf16[640,2048]{1,0:T(8,128)(2,1)} %bitcast.12, bf16[1,2048,896]{2,1,0:T(8,128)(2,1)} %param.23), kind=kOutput, calls=%fused_computation.11 | convolution fusion | flops 2348810240 | bytes 8585216 | tf_op jit(solution)/shard_map/dot_general | solution.py:86
  103.2 0.0 copy-start.2
  103.2 11.8 %fusion.12 = bf16[640,2048]{1,0:T(8,128)(2,1)} fusion(bf16[1,896,2048]{2,1,0:T(8,128)(2,1)} %param.25, f32[640,896]{1,0:T(8,128)} %fusion.10, bf16[640,2048]{1,0:T(8,128)(2,1)} %bitcast.12, bf16[1,2048,896]{2,1,0:T(8,128)(2,1)} %param.24), kind=kOutput, calls=%fused_computation.13 | convolution fusion | flops 4702371840 | bytes 14876672 | tf_op jit(solution)/shard_map/dot_general | solution.py:89
  115.0 0.0 reduce-scatter.5.cloned.1.call-update
  115.0 0.2 reduce-scatter.3.cloned.1.call-start
  115.3 0.0 copy-done.2
  115.3 0.1 copy.39
  115.4 0.4 iota_compare_fusion
  115.8 0.0 all-gather.3.cloned.1.call-done
  115.8 1.5 copy.40
  117.3 11.8 %all-gather.5.cloned.1.call-done = bf16[2048,256]{1,0:T(8,128)(2,1)} async-done(((bf16[256,256]{1,0:T(8,128)(2,1)}), bf16[2048,256]{1,0:T(8,128)(2,1)}) %all-gather.5.cloned.1.call-update) | async-done | bytes 1048592 | tf_op jit(solution)/shard_map/all_gather | solution.py:19
  129.1 2.3 %copy.41 = bf16[2048,256]{0,1:T(8,128)(2,1)} copy(bf16[2048,256]{1,0:T(8,128)(2,1)} %all-gather.5.cloned.1.call-done) | data formatting | bytes 2097152 | tf_op jit(solution)/shard_map/all_gather | solution.py:19
  131.3 1.8 fusion
  133.1 0.0 copy-start.1
  133.1 2.5 %fusion.1 = f32[2,2,256]{2,1,0:T(2,128)S(1)} fusion(f32[2,2,256,2048]{3,2,1,0:T(8,128)S(1)} %get-tuple-element.3, f32[2,2,256]{2,1,0:T(2,128)S(1)} %broadcast_maximum_fusion, pred[256,2048]{1,0:T(8,128)(4,1)S(1)} %iota_compare_fusion), kind=kLoop, calls=%fused_computation.3 | loop fusion | flops 10484736 | bytes 8921088 | tf_op jit(solution)/shard_map/reduce_sum | solution.py:31
  135.6 0.0 copy-done.1
  135.6 0.0 copy-start.4
  135.6 0.0 copy-start.5
  135.6 2.2 %fusion.20 = f32[2,2,256,128]{2,3,1,0:T(8,128)S(1)} fusion(bf16[2048,2,128,1]{0,2,3,1:T(8,128)(2,1)S(1)} %bitcast.71, f32[2,2,256,2048]{3,2,1,0:T(8,128)S(1)} %get-tuple-element.3, f32[2,2,256]{2,1,0:T(2,128)S(1)} %broadcast_maximum_fusion, pred[256,2048]{1,0:T(8,128)(4,1)S(1)} %iota_compare_fusion, f32[2,2,256]{2,1,0:T(2,128)S(1)} %fusion.1), kind=kOutput, calls=%fused_computation.24 | convolution fusion | flops 547487744 | bytes 10493952 | tf_op jit(solution)/shard_map/hmqk,khd->hmqd/dot_general | solution.py:32
  137.9 0.0 copy-done.4
  137.9 0.0 copy-start.3
  137.9 0.1 multiply_reduce_fusion
  138.0 0.0 copy-done.5
  138.1 0.1 multiply_convert_fusion.1
  138.2 0.0 copy-done
  138.2 1.5 convolution_convert_fusion.1
  139.6 0.0 reduce-scatter.3.cloned.1.call-update
  139.7 8.8 %reduce-scatter.5.cloned.1.call-done = bf16[640,512]{1,0:T(8,128)(2,1)} async-done(((bf16[640,2048]{1,0:T(8,128)(2,1)}), bf16[640,512]{1,0:T(8,128)(2,1)}) %reduce-scatter.5.cloned.1.call-update) | async-done | bytes 655376 | tf_op jit(solution)/shard_map/reduce_scatter | solution.py:90
  148.5 5.5 %all-to-all-start.1 = ((bf16[8,80,512]{2,1,0:T(8,128)(2,1)}), bf16[8,80,512]{2,1,0:T(8,128)(2,1)S(1)}, u32[]{:S(2)}, u32[]{:S(2)}) async-start(bf16[8,80,512]{2,1,0:T(8,128)(2,1)} %bitcast.72), calls=%async_computation.3 | async-start | bytes 1310720 | tf_op jit(solution)/shard_map/all_to_all | solution.py:94
  154.0 0.0 copy-done.3
  154.0 0.2 select_reduce_fusion
  154.2 16.9 %all-to-all-done.1 = bf16[8,80,512]{2,1,0:T(8,128)(2,1)S(1)} async-done(((bf16[8,80,512]{2,1,0:T(8,128)(2,1)}), bf16[8,80,512]{2,1,0:T(8,128)(2,1)S(1)}, u32[]{:S(2)}, u32[]{:S(2)}) %all-to-all-start.1) | async-done | bytes 655392 | tf_op jit(solution)/shard_map/all_to_all | solution.py:94
  171.1 1.3 convolution_convert_fusion.2
  172.4 3.9 %reduce-scatter.3.cloned.1.call-done = bf16[64,2048]{1,0:T(8,128)(2,1)} async-done(((bf16[256,2048]{1,0:T(8,128)(2,1)}), bf16[64,2048]{1,0:T(8,128)(2,1)}) %reduce-scatter.3.cloned.1.call-update) | async-done | bytes 262160 | tf_op jit(solution)/shard_map/reduce_scatter | solution.py:45
  (6 shorter events, 0.1 us)
Async XLA Ops:
  8.0 130.2 %copy-start = (bf16[256,2048]{1,0:T(8,128)(2,1)S(1)}, bf16[256,2048]{1,0:T(8,128)(2,1)}, u32[]{:S(2)}) copy-start(bf16[256,2048]{1,0:T(8,128)(2,1)} %param.18) | copy-start | bytes 3145732
  16.5 79.5 %all-to-all-start = ((bf16[8,80,2048]{2,1,0:T(8,128)(2,1)}), bf16[8,80,2048]{2,1,0:T(8,128)(2,1)}, u32[]{:S(2)}, u32[]{:S(2)}) async-start(bf16[8,80,2048]{2,1,0:T(8,128)(2,1)} %bitcast.68), calls=%async_computation.1 | async-start | bytes 5242880 | tf_op jit(solution)/shard_map/all_to_all | solution.py:79
  23.8 92.0 %all-gather.3.cloned.1.call-start = ((), (), s32[]{:S(2)}) async-start(), calls=%async_computation.4 | async-start | bytes 1179648 | tf_op jit(solution)/shard_map/all_gather | solution.py:18
  24.5 104.6 %all-gather.5.cloned.1.call-start = ((), (), s32[]{:S(2)}) async-start(), calls=%async_computation.5 | async-start | bytes 1179648 | tf_op jit(solution)/shard_map/all_gather | solution.py:19
  25.3 123.2 %reduce-scatter.5.cloned.1.call-start = ((), (), s32[]{:S(2)}) async-start(), calls=%async_computation.7 | async-start | bytes 3276800 | tf_op jit(solution)/shard_map/reduce_scatter | solution.py:90
  103.2 12.1 %copy-start.2 = (bf16[256,256]{1,0:T(8,128)(2,1)S(1)}, bf16[256,256]{1,0:T(8,128)(2,1)}, u32[]{:S(2)}) copy-start(bf16[256,256]{1,0:T(8,128)(2,1)} %param.13) | copy-start | bytes 393220
  115.0 61.2 %reduce-scatter.3.cloned.1.call-start = ((), (), s32[]{:S(2)}) async-start(), calls=%async_computation.6 | async-start | bytes 1310720 | tf_op jit(solution)/shard_map/reduce_scatter | solution.py:45
  133.1 2.5 %copy-start.1 = (bf16[2048,256]{0,1:T(8,128)(2,1)S(1)}, bf16[2048,256]{0,1:T(8,128)(2,1)}, u32[]{:S(2)}) copy-start(bf16[2048,256]{0,1:T(8,128)(2,1)} %copy.41) | copy-start | bytes 3145732
  135.6 2.3 %copy-start.4 = (f32[2]{0:T(128)S(1)}, f32[2]{0:T(128)}, u32[]{:S(2)}) copy-start(f32[2]{0:T(128)} %param.16) | copy-start | bytes 28
  135.6 2.4 %copy-start.5 = (f32[128]{0:T(128)S(1)}, f32[128]{0:T(128)}, u32[]{:S(2)}) copy-start(f32[128]{0:T(128)} %param.17) | copy-start | bytes 1540
  137.9 16.1 %copy-start.3 = (f32[192,2]{0,1:T(2,128)S(1)}, f32[192,2]{0,1:T(2,128)}, u32[]{:S(2)}) copy-start(f32[192,2]{0,1:T(2,128)} %param.22) | copy-start | bytes 4612
  148.5 22.6 %all-to-all-start.1 = ((bf16[8,80,512]{2,1,0:T(8,128)(2,1)}), bf16[8,80,512]{2,1,0:T(8,128)(2,1)S(1)}, u32[]{:S(2)}, u32[]{:S(2)}) async-start(bf16[8,80,512]{2,1,0:T(8,128)(2,1)} %bitcast.72), calls=%async_computation.3 | async-start | bytes 1310720 | tf_op jit(solution)/shard_map/all_to_all | solution.py:94
Sparse Core Ops, SparseCore 0:
  26.7 60.7 all-gather.2
  89.7 39.3 all-gather.4
Sparse Core Ops, SparseCore 1:
  115.1 33.3 reduce-scatter.4
  151.5 24.7 reduce-scatter.2
where the time goes:
time: 184 us
  waiting for transfers between devices  113 us (61%)
  matrix products  29.4 us (16%)
  between operations  15.7 us (9%)
  starting transfers between devices  13.2 us (7%)
  other arithmetic  6.48 us (4%)
  local copies, waits for them, and re-layouts  5.48 us (3%)
    all_to_all x1, waiting for transfers between devices, expert_half(): lax.all_to_all(outgoing.reshape(experts, capacity, model_width), 'ep', sp...  70.7 us
    all_to_all x1, waiting for transfers between devices, expert_half(): lax.all_to_all(summed.reshape(experts, capacity, col_count), 'ep', split_...  16.9 us
    dot_general x1, matrix products, expert_half(): jnp.dot(hidden, down_mat, preferred_element_type=jnp.float32)  11.8 us
    all_gather x1, waiting for transfers between devices, mixer_half(): value_piece = lax.all_gather(value_rows, 'ep', axis=0, tiled=True)  11.8 us
    reduce_scatter x1, waiting for transfers between devices, expert_half(): lax.psum_scatter(partial_result.astype(jnp.bfloat16), 'tp', scatter_dimen...  8.83 us
    all_to_all x1, starting transfers between devices, expert_half(): lax.all_to_all(outgoing.reshape(experts, capacity, model_width), 'ep', sp...  7.28 us
    dot_general x1, matrix products, expert_half(): gate_act = jnp.dot(arrived, gate_mat, preferred_element_type=jnp.float32)  7.18 us
    all_to_all x1, starting transfers between devices, expert_half(): lax.all_to_all(summed.reshape(experts, capacity, col_count), 'ep', split_...  5.54 us
  transfers between devices with their start and end apart: 6, of which 5 were waited for; matrix products, arithmetic and copies ran while one was open for 18% of the time, Pallas kernels for 0%

commit v1 on v0

--- a/solution.py
+++ b/solution.py
@@ -15,8 +15,11 @@
     query_blocks = queries.reshape(rows_here, heads_here, 2, head_width)
     query_pos = lax.axis_index("ep") * rows_here + jnp.arange(rows_here, dtype=jnp.int32)
     row_max = jnp.full((heads_here, 2, rows_here), -1e30, jnp.float32)
-    key_piece = lax.all_gather(key_rows, "ep", axis=0, tiled=True)
-    value_piece = lax.all_gather(value_rows, "ep", axis=0, tiled=True)
+    key_piece, value_piece = jnp.split(
+        lax.all_gather(jnp.concatenate([key_rows, value_rows], axis=1), "ep", axis=0, tiled=True),
+        [key_rows.shape[1]],
+        axis=1,
+    )
     length = key_piece.shape[0]
     key_blocks = key_piece.reshape(length, heads_here, 2, head_width)
     value_blocks = value_piece.reshape(length, heads_here, value_width)

time: 184 us -> 197 us (1.071)
  waiting for transfers between devices: 113 us -> 124 us
    all_to_all x1, waiting for transfers between devices: 70.7 us -> 84 us  [expert_half(): lax.all_to_all(outgoing.reshape(experts, capacity, model_width), 'ep', sp...]
    all_gather x2 -> x1, waiting for transfers between devices: 11.8 us -> 0.01 us  [mixer_half(): lax.all_gather(jnp.concatenate([key_rows, value_rows], axis=1), 'ep', axi...]
    reduce_scatter x1, waiting for transfers between devices: 8.83 us -> 19.5 us  [expert_half(): lax.psum_scatter(partial_result.astype(jnp.bfloat16), 'tp', scatter_dimen...]
    all_gather x2 -> x0, local copies, waits for them, and re-layouts: 3.75 us -> none  [the longest x1 2.26 us: mixer_half(): value_piece = lax.all_gather(value_rows, 'ep', axis=0, tiled=True)]
    split x0 -> x3, local copies, waits for them, and re-layouts: none -> 3.73 us  [mixer_half(): jnp.split(lax.all_gather(jnp.concatenate([key_rows, value_rows], axis=1),...]
  transfers between devices with their start and end apart: 6 -> 5, of which waited for: 5 -> 4; matrix products, arithmetic and copies ran while one was open for 18% -> 18% of each run, Pallas kernels for 0% -> 0%
where the time goes in v1:
time: 197 us; the launch traced here: 196 us
  waiting for transfers between devices  124 us (63%)
  matrix products  30.1 us (15%)
  between operations  15.7 us (8%)
  starting transfers between devices  13.1 us (7%)
  other arithmetic  7.61 us (4%)
  local copies, waits for them, and re-layouts  5.48 us (3%)
    all_to_all x1, waiting for transfers between devices, expert_half(): lax.all_to_all(outgoing.reshape(experts, capacity, model_width), 'ep', sp...  84 us
    reduce_scatter x1, waiting for transfers between devices, expert_half(): lax.psum_scatter(partial_result.astype(jnp.bfloat16), 'tp', scatter_dimen...  19.5 us
    all_to_all x1, waiting for transfers between devices, expert_half(): lax.all_to_all(summed.reshape(experts, capacity, col_count), 'ep', split_...  16.9 us
    dot_general x1, matrix products, expert_half(): jnp.dot(hidden, down_mat, preferred_element_type=jnp.float32)  11.8 us
    all_to_all x1, starting transfers between devices, expert_half(): lax.all_to_all(outgoing.reshape(experts, capacity, model_width), 'ep', sp...  7.28 us
    dot_general x1, matrix products, expert_half(): gate_act = jnp.dot(arrived, gate_mat, preferred_element_type=jnp.float32)  7.11 us
    all_to_all x1, starting transfers between devices, expert_half(): lax.all_to_all(summed.reshape(experts, capacity, col_count), 'ep', split_...  5.51 us
  transfers between devices with their start and end apart: 5, of which 4 were waited for; matrix products, arithmetic and copies ran while one was open for 18% of the time, Pallas kernels for 0%

profile of v1, /device:TPU:0, one launch (start us, length us, event | category | flops | bytes accessed | tf_op | source)
XLA Modules:
  0.0 196.3 jit_solution(18286470993204731699)
XLA Ops:
  8.0 0.0 copy-start
  8.0 0.9 copy.47
  8.9 0.1 eq.42
  9.0 0.1 eq.38
  9.2 0.9 reduce-window.6
  10.1 0.2 slice_reduce_fusion
  10.3 0.1 fusion.32
  10.4 0.1 reduce_sum.50
  10.6 0.1 copy.49
  10.6 0.7 multiply_add_fusion
  11.3 0.1 fusion.23
  11.5 1.4 fusion.17
  12.9 0.0 copy-start.4
  12.9 0.0 copy-start.5
  12.9 3.6 %convolution_convert_fusion = bf16[640,2048]{1,0:T(8,128)(2,1)} fusion(pred[640,192]{0,1:T(8,128)(4,1)S(1)} %fusion.23, bf16[192,2048]{1,0:T(8,128)(2,1)} %param.19, f32[2048]{0:T(1024)} %param.20, f32[192]{0:T(256)S(1)} %add_rsqrt_fusion.1), kind=kOutput, calls=%fused_computation.14 | convolution fusion | flops 506200064 | bytes 3539712 | tf_op jit(solution)/shard_map/dot_general | solution.py:81
  16.5 7.3 %all-to-all-start = ((bf16[8,80,2048]{2,1,0:T(8,128)(2,1)}), bf16[8,80,2048]{2,1,0:T(8,128)(2,1)}, u32[]{:S(2)}, u32[]{:S(2)}) async-start(bf16[8,80,2048]{2,1,0:T(8,128)(2,1)} %bitcast.81), calls=%async_computation.1 | async-start | bytes 5242880 | tf_op jit(solution)/shard_map/all_to_all | solution.py:82
  23.8 0.0 all-gather.2.cloned.1.call-start
  23.9 0.0 copy-done.4
  23.9 0.0 copy-done.5
  23.9 0.7 pad_maximum_fusion
  24.6 0.0 all-gather.2.cloned.1.call-update
  24.6 0.0 reduce-scatter.5.cloned.1.call-start
  24.7 84.0 %all-to-all-done = bf16[8,80,2048]{2,1,0:T(8,128)(2,1)} async-done(((bf16[8,80,2048]{2,1,0:T(8,128)(2,1)}), bf16[8,80,2048]{2,1,0:T(8,128)(2,1)}, u32[]{:S(2)}, u32[]{:S(2)}) %all-to-all-start) | async-done | bytes 2621472 | tf_op jit(solution)/shard_map/all_to_all | solution.py:82
  108.7 7.1 %fusion.10 = f32[640,896]{1,0:T(8,128)} fusion(bf16[640,2048]{1,0:T(8,128)(2,1)} %bitcast.13, bf16[1,2048,896]{2,1,0:T(8,128)(2,1)} %param.23), kind=kOutput, calls=%fused_computation.11 | convolution fusion | flops 2348810240 | bytes 8585216 | tf_op jit(solution)/shard_map/dot_general | solution.py:89
  115.8 0.0 copy-start.3
  115.8 11.8 %fusion.12 = bf16[640,2048]{1,0:T(8,128)(2,1)} fusion(bf16[1,896,2048]{2,1,0:T(8,128)(2,1)} %param.25, f32[640,896]{1,0:T(8,128)} %fusion.10, bf16[640,2048]{1,0:T(8,128)(2,1)} %bitcast.13, bf16[1,2048,896]{2,1,0:T(8,128)(2,1)} %param.24), kind=kOutput, calls=%fused_computation.13 | convolution fusion | flops 4702371840 | bytes 14876672 | tf_op jit(solution)/shard_map/dot_general | solution.py:92
  127.6 0.0 reduce-scatter.5.cloned.1.call-update
  127.6 0.2 reduce-scatter.3.cloned.1.call-start
  127.8 0.0 copy-done.3
  127.9 0.1 copy.43
  128.0 1.1 iota_compare_fusion
  129.1 0.0 all-gather.2.cloned.1.call-done
  129.1 1.7 fusion.38
  130.8 1.4 copy.44
  132.2 0.6 copy.42
  132.9 0.0 copy-start.1
  132.9 2.7 %fusion = (f32[2,2,256]{2,1,0:T(2,128)S(1)}, f32[2,2,2048,256]{3,2,1,0:T(8,128)S(1)}) fusion(pred[256,2048]{0,1:T(8,128)(4,1)} %iota_compare_fusion, bf16[2048,2,2,64]{0,3,2,1:T(8,128)(2,1)S(1)} %bitcast.84, bf16[256,2,2,64]{0,3,2,1:T(8,128)(2,1)S(1)} %bitcast.87), kind=kOutput, calls=%fused_computation.2 | convolution fusion | flops 274725888 | bytes 10096640 | tf_op jit(solution)/shard_map/qhmd,khmd->hmqk/dot_general | solution.py:27
  135.6 0.0 copy-done.1
  135.6 0.0 copy-start.2
  135.6 2.1 %fusion.1 = f32[2,2,256]{2,1,0:T(2,128)S(1)} fusion(f32[2,2,2048,256]{3,2,1,0:T(8,128)S(1)} %get-tuple-element.5, f32[2,2,256]{2,1,0:T(2,128)S(1)} %broadcast_maximum_fusion, pred[256,2048]{0,1:T(8,128)(4,1)S(1)} %copy-done.1), kind=kLoop, calls=%fused_computation.3 | loop fusion | flops 10484736 | bytes 8921088 | tf_op jit(solution)/shard_map/reduce_sum | solution.py:34
  137.7 0.0 copy-done.2
  137.7 0.0 copy-start.7
  137.8 0.0 copy-start.8
  137.8 2.1 %fusion.20 = f32[2,2,256,128]{2,3,1,0:T(8,128)S(1)} fusion(bf16[2048,2,128,1]{0,2,3,1:T(8,128)(2,1)S(1)} %bitcast.83, f32[2,2,2048,256]{3,2,1,0:T(8,128)S(1)} %get-tuple-element.5, f32[2,2,256]{2,1,0:T(2,128)S(1)} %broadcast_maximum_fusion, pred[256,2048]{0,1:T(8,128)(4,1)S(1)} %copy-done.1, f32[2,2,256]{2,1,0:T(2,128)S(1)} %fusion.1), kind=kOutput, calls=%fused_computation.24 | convolution fusion | flops 547487744 | bytes 10493952 | tf_op jit(solution)/shard_map/hmqk,khd->hmqd/dot_general | solution.py:35
  139.9 0.0 copy-done.7
  139.9 0.0 copy-start.6
  139.9 0.1 multiply_reduce_fusion
  140.0 0.0 copy-done.8
  140.0 0.1 multiply_convert_fusion.1
  140.2 0.0 copy-done
  140.2 1.5 convolution_convert_fusion.1
  141.6 0.0 reduce-scatter.3.cloned.1.call-update
  141.6 19.5 %reduce-scatter.5.cloned.1.call-done = bf16[640,512]{1,0:T(8,128)(2,1)} async-done(((bf16[640,2048]{1,0:T(8,128)(2,1)}), bf16[640,512]{1,0:T(8,128)(2,1)}) %reduce-scatter.5.cloned.1.call-update) | async-done | bytes 655376 | tf_op jit(solution)/shard_map/reduce_scatter | solution.py:93
  161.1 5.5 %all-to-all-start.1 = ((bf16[8,80,512]{2,1,0:T(8,128)(2,1)}), bf16[8,80,512]{2,1,0:T(8,128)(2,1)S(1)}, u32[]{:S(2)}, u32[]{:S(2)}) async-start(bf16[8,80,512]{2,1,0:T(8,128)(2,1)} %bitcast.85), calls=%async_computation.3 | async-start | bytes 1310720 | tf_op jit(solution)/shard_map/all_to_all | solution.py:97
  166.6 0.0 copy-done.6
  166.6 0.2 select_reduce_fusion
  166.8 16.9 %all-to-all-done.1 = bf16[8,80,512]{2,1,0:T(8,128)(2,1)S(1)} async-done(((bf16[8,80,512]{2,1,0:T(8,128)(2,1)}), bf16[8,80,512]{2,1,0:T(8,128)(2,1)S(1)}, u32[]{:S(2)}, u32[]{:S(2)}) %all-to-all-start.1) | async-done | bytes 655392 | tf_op jit(solution)/shard_map/all_to_all | solution.py:97
  183.7 1.3 convolution_convert_fusion.2
  185.0 3.8 %reduce-scatter.3.cloned.1.call-done = bf16[64,2048]{1,0:T(8,128)(2,1)} async-done(((bf16[256,2048]{1,0:T(8,128)(2,1)}), bf16[64,2048]{1,0:T(8,128)(2,1)}) %reduce-scatter.3.cloned.1.call-update) | async-done | bytes 262160 | tf_op jit(solution)/shard_map/reduce_scatter | solution.py:48
  (6 shorter events, 0.1 us)
Async XLA Ops:
  8.0 132.2 %copy-start = (bf16[256,2048]{1,0:T(8,128)(2,1)S(1)}, bf16[256,2048]{1,0:T(8,128)(2,1)}, u32[]{:S(2)}) copy-start(bf16[256,2048]{1,0:T(8,128)(2,1)} %param.18) | copy-start | bytes 3145732
  12.9 11.0 %copy-start.4 = (bf16[256,256]{1,0:T(8,128)(2,1)S(1)}, bf16[256,256]{1,0:T(8,128)(2,1)}, u32[]{:S(2)}) copy-start(bf16[256,256]{1,0:T(8,128)(2,1)} %param.15) | copy-start | bytes 393220
  12.9 11.0 %copy-start.5 = (bf16[256,256]{1,0:T(8,128)(2,1)S(1)}, bf16[256,256]{1,0:T(8,128)(2,1)}, u32[]{:S(2)}) copy-start(bf16[256,256]{1,0:T(8,128)(2,1)} %param.14) | copy-start | bytes 393220
  16.5 92.1 %all-to-all-start = ((bf16[8,80,2048]{2,1,0:T(8,128)(2,1)}), bf16[8,80,2048]{2,1,0:T(8,128)(2,1)}, u32[]{:S(2)}, u32[]{:S(2)}) async-start(bf16[8,80,2048]{2,1,0:T(8,128)(2,1)} %bitcast.81), calls=%async_computation.1 | async-start | bytes 5242880 | tf_op jit(solution)/shard_map/all_to_all | solution.py:82
  23.8 105.3 %all-gather.2.cloned.1.call-start = ((), (), s32[]{:S(2)}) async-start(), calls=%async_computation.4 | async-start | bytes 2359296 | tf_op jit(solution)/shard_map/all_gather | solution.py:19
  24.6 136.5 %reduce-scatter.5.cloned.1.call-start = ((), (), s32[]{:S(2)}) async-start(), calls=%async_computation.6 | async-start | bytes 3276800 | tf_op jit(solution)/shard_map/reduce_scatter | solution.py:93
  115.8 12.0 %copy-start.3 = (bf16[256,256]{1,0:T(8,128)(2,1)S(1)}, bf16[256,256]{1,0:T(8,128)(2,1)}, u32[]{:S(2)}) copy-start(bf16[256,256]{1,0:T(8,128)(2,1)} %param.13) | copy-start | bytes 393220
  127.6 61.3 %reduce-scatter.3.cloned.1.call-start = ((), (), s32[]{:S(2)}) async-start(), calls=%async_computation.5 | async-start | bytes 1310720 | tf_op jit(solution)/shard_map/reduce_scatter | solution.py:48
  132.9 2.8 %copy-start.1 = (pred[256,2048]{0,1:T(8,128)(4,1)S(1)}, pred[256,2048]{0,1:T(8,128)(4,1)}, u32[]{:S(2)}) copy-start(pred[256,2048]{0,1:T(8,128)(4,1)} %iota_compare_fusion) | copy-start | bytes 1572868
  135.6 2.1 %copy-start.2 = (bf16[2048,256]{0,1:T(8,128)(2,1)S(1)}, bf16[2048,256]{0,1:T(8,128)(2,1)}, u32[]{:S(2)}) copy-start(bf16[2048,256]{0,1:T(8,128)(2,1)} %copy.44) | copy-start | bytes 3145732
  137.7 2.1 %copy-start.7 = (f32[2]{0:T(128)S(1)}, f32[2]{0:T(128)}, u32[]{:S(2)}) copy-start(f32[2]{0:T(128)} %param.16) | copy-start | bytes 28
  137.8 2.3 %copy-start.8 = (f32[128]{0:T(128)S(1)}, f32[128]{0:T(128)}, u32[]{:S(2)}) copy-start(f32[128]{0:T(128)} %param.17) | copy-start | bytes 1540
  139.9 26.7 %copy-start.6 = (f32[192,2]{0,1:T(2,128)S(1)}, f32[192,2]{0,1:T(2,128)}, u32[]{:S(2)}) copy-start(f32[192,2]{0,1:T(2,128)} %param.22) | copy-start | bytes 4612
  161.1 22.6 %all-to-all-start.1 = ((bf16[8,80,512]{2,1,0:T(8,128)(2,1)}), bf16[8,80,512]{2,1,0:T(8,128)(2,1)S(1)}, u32[]{:S(2)}, u32[]{:S(2)}) async-start(bf16[8,80,512]{2,1,0:T(8,128)(2,1)} %bitcast.85), calls=%async_computation.3 | async-start | bytes 1310720 | tf_op jit(solution)/shard_map/all_to_all | solution.py:97
Sparse Core Ops, SparseCore 0:
  27.3 81.9 all-gather.1
Sparse Core Ops, SparseCore 1:
  127.7 33.4 reduce-scatter.4
  164.1 24.7 reduce-scatter.2
